TPU v7x, 512 devices: a whole 4x8x8 slice. The times are simulated.
512 devices in a mesh: sp: 64 (over z, y), tp: 8 (over x, core).
Axes of the slice: x: 4, y: 8, z: 8, core: 2. Of those that a mesh axis runs over, the one named last changes fastest.
Arguments:
- tokens: bfloat16 [16384, 2048], P('sp', 'tp'), may hold values from -24 to 24
- value_weight: bfloat16 [2, 2048, 2048], P(None, 'sp', 'tp'), may hold values from -0.125 to 0.125
- outer_weight: bfloat16 [2, 2048, 2048], P(None, 'sp', 'tp'), may hold values from -0.125 to 0.125
- inner_weight: bfloat16 [2, 2048, 2048], P(None, 'sp', 'tp'), may hold values from -0.125 to 0.125
- conv_taps: float32 [2, 3, 2048], P(None, None, 'tp'), may hold values from -3.5 to 3.5
- output_weight: bfloat16 [2, 2048, 2048], P(None, 'tp', 'sp'), may hold values from -2 to 2
- norm_gain: float32 [2, 2048], P(None, 'tp'), may hold values from 0.1 to 1.9
- norm_bias: float32 [2, 2048], P(None, 'tp'), may hold values from -3 to 3
Outputs:
- mixed_out: bfloat16 [16384, 2048], P('sp', 'tp')
All inputs are finite; a program needn't handle non-finite values.
Results may differ from a plain program's by a relative error of at most 0.03.
Values may be sent and summed in bfloat16 or wider, within the bound.
No kernel may reach another device: no remote copies, remote signals or barrier semaphores. Data moves between devices by JAX's collectives and lax.ppermute only.
A program may use at most 64 MiB of HBM per device.

v0:
```python
import jax
import jax.numpy as jnp
from jax import lax
from jax.sharding import Mesh, PartitionSpec as P

D = 2048
LAYERS = 2
TP = ("x", "core")
SP = ("z", "y")
HALO = 16
IN_UP, OUT_UP = (2.0**18, 2.0**14)


def bf(x):
    return x.astype(jnp.bfloat16)


def f32(x):
    return x.astype(jnp.float32)


def rounded(x):
    return lax.reduce_precision(x, exponent_bits=8, mantissa_bits=7)


def thirds(x):
    a = rounded(x)
    b = rounded(x - a)
    c = rounded(x - a - b)
    return jnp.stack([bf(a), bf(b), bf(c)])


def packed(value, outer, inner, out, layer):
    return jnp.concatenate([value[layer], outer[layer], inner[layer], out[layer].T], axis=1)


def norm(pre, gain, bias):
    mean = jnp.mean(pre, axis=-1, keepdims=True)
    cent = pre - mean
    var = jnp.mean(cent * cent, axis=-1, keepdims=True)
    return bf(cent * lax.rsqrt(var + 1e-05) * gain + bias)


def gated_rows(x, w_in, down, taps, first, head):
    width = w_in.shape[1] // 3
    acc = jnp.dot(x, w_in, preferred_element_type=jnp.float32) * down
    u, outer, inner = (f32(bf(acc[:, i * width : (i + 1) * width])) for i in range(3))
    z = inner * u
    row = lax.broadcasted_iota(jnp.int32, z.shape, 0)
    z = jnp.where(jnp.logical_and(first, row < head), 0.0, z)
    conv = taps[2] * z[2:] + taps[1] * z[1:-1] + taps[0] * z[:-2]
    return bf(outer[2:] * conv)


def out_product(g, w_out_t, down):
    return (
        lax.dot_general(g, w_out_t, (((1,), (1,)), ((), ())), preferred_element_type=jnp.float32)
        * down
    )


def pair_sum(main, extra, w_out_t, down, core):
    blocks = main.reshape(4, 2, 32, -1)
    mine = jnp.where(core == 0, blocks[:, 0], blocks[:, 1]).reshape(128, -1)
    other = jnp.where(core == 0, blocks[:, 1], blocks[:, 0]).reshape(128, -1)
    if extra is not None:
        mine = jnp.concatenate([mine, extra], axis=0)
        other = jnp.concatenate([other, extra], axis=0)
    sent = bf(out_product(other, w_out_t, down))
    got = lax.ppermute(sent, "core", [(0, 1), (1, 0)])
    return out_product(mine, w_out_t, down) + f32(got)


def shards(tokens, value, outer, inner, taps, out, gain, bias):
    alpha = (2.0 * LAYERS) ** 0.25
    core = lax.axis_index("core")
    sp = lax.axis_index(SP)
    tp = lax.axis_index(TP)
    first = sp == 0
    late = lax.all_gather(packed(value, outer, inner, out, 1), SP, axis=0, tiled=True)
    halo = lax.ppermute(tokens[-HALO:], SP, [(i, i + 1) for i in range(63)])
    params = jnp.concatenate([gain, bias], axis=0)
    parts = thirds(params).reshape(12, 256)
    parts = jnp.concatenate([parts, jnp.zeros((4, 256), jnp.bfloat16)], axis=0)
    mine = jnp.concatenate([halo, tokens, parts], axis=0)
    everyone = lax.all_to_all(jnp.broadcast_to(mine[None], (8, *mine.shape)), TP, 0, 0, tiled=True)
    scale = jnp.where(jnp.arange(1024) < 768, IN_UP, OUT_UP)
    early = (f32(packed(value, outer, inner, out, 0)) * scale).astype(jnp.float16)
    early = lax.all_gather(early, SP, axis=0, tiled=True)
    early = bf(early)
    whole = jnp.moveaxis(everyone, 0, 1).reshape(288, D)
    table = f32(whole[272:284]).reshape(3, 4, D)
    table = table[0] + table[1] + table[2]
    x0 = whole[:272]
    g = gated_rows(x0, early[:, :768], 1.0 / IN_UP, taps[0], first, HALO)
    branch = pair_sum(g[HALO - 2 :], g[HALO - 10 : HALO - 2], early[:, 768:], 1.0 / OUT_UP, core)
    main = bf(branch[:128]).reshape(4, 32, D)
    extra = bf(branch[134:136]).reshape(32, 128)
    send = jnp.concatenate([main, jnp.broadcast_to(extra[None], (4, 32, 128))], axis=2)
    got = jnp.sum(f32(lax.all_to_all(send, "x", 0, 0, tiled=True)), axis=0)
    own = lax.dynamic_slice_in_dim(x0, HALO + 32 * tp, 32, axis=0)
    pre = jnp.concatenate(
        [
            alpha * f32(own) + got[:, :D],
            alpha * f32(x0[HALO - 2 : HALO]) + got[:, D:].reshape(2, D),
        ],
        axis=0,
    )
    state = norm(pre, table[0], table[2])
    own = state[:32]
    every = lax.all_gather(own.astype(jnp.float16), TP, axis=0, tiled=True)
    x1 = jnp.concatenate([jnp.zeros((6, D), jnp.bfloat16), state[32:], bf(every)], axis=0)
    g = gated_rows(x1, late[:, :768], 1.0, taps[1], first, 8)
    branch = pair_sum(g[6:], None, late[:, 768:], 1.0, core)
    got = lax.all_to_all(bf(branch).reshape(4, 32, D), "x", 0, 0, tiled=True)
    pre = alpha * f32(own) + jnp.sum(f32(got), axis=0)
    state = norm(pre, table[1], table[3])
    back = jnp.moveaxis(state.reshape(32, 8, 256), 1, 0)
    return lax.all_to_all(back, TP, 0, 0, tiled=True).reshape(256, 256)


def solution(mesh):
    mesh = Mesh(mesh.devices.reshape(8, 8, 4, 2), ("z", "y", "x", "core"))
    in_specs = (
        P(SP, TP),
        P(None, SP, TP),
        P(None, SP, TP),
        P(None, SP, TP),
        P(None, None, TP),
        P(None, TP, SP),
        P(None, TP),
        P(None, TP),
    )
    return jax.shard_map(shards, mesh=mesh, in_specs=in_specs, out_specs=P(SP, TP), check_vma=False)
```

profile of v0, /device:TPU:1, one launch (start us, length us, event | category | flops | bytes accessed | tf_op | source)
XLA Modules:
  0.0 170.9 jit_solution(12494518444327532426)
XLA Ops:
  6.5 0.7 slice_bitcast_fusion.8
  7.3 0.7 slice_bitcast_fusion.5
  8.0 0.8 slice_bitcast_fusion.6
  8.8 0.6 pad_maximum_fusion.6
  9.4 0.7 slice.214
  10.1 4.0 %collective-permute-start = (bf16[16,256]{1,0:T(8,128)(2,1)S(1)}, bf16[16,256]{1,0:T(8,128)(2,1)S(1)}, u32[]{:S(2)}, u32[]{:S(2)}) collective-permute-start(bf16[16,256]{1,0:T(8,128)(2,1)S(1)} %slice.214), channel_id=1, source_target_pairs={{0,8},{8,16},{16,24},{24,32},{32,40},{40,48},{48,56},{56,64},{64,7... | collective-permute-start | bytes 24584 | tf_op jit(solution)/shard_map/ppermute | solution.py:81
  14.2 0.7 reduce-precision_convert_fusion.1
  15.0 1.0 maximum_maximum_fusion
  16.1 1.2 broadcast_in_dim.41
  17.2 8.0 %all-to-all-start = ((bf16[8,288,256]{2,1,0:T(8,128)(2,1)}), bf16[8,288,256]{2,1,0:T(8,128)(2,1)S(1)}, u32[]{:S(2)}, u32[]{:S(2)}) async-start(bf16[8,288,256]{2,1,0:T(8,128)(2,1)} %broadcast_in_dim.41), calls=%async_computation | async-start | bytes 2359296 | tf_op jit(solution)/shard_map/all_to_all | solution.py:86
  25.3 56.9 %all-gather.5 = f16[2048,1024]{1,0:T(8,128)(2,1)S(1)} all-gather(f16[32,1024]{1,0:T(8,128)(2,1)S(1)} %multiply_convert_fusion), channel_id=1, replica_groups=mesh['z'=8,'y'=8,'x'=4,'core'=2] {'z','y'}, dimensions={0}, use_global_device_ids=true | all-gather | bytes 4259840 | tf_op jit(solution)/shard_map/all_gather | solution.py:89
  82.2 3.2 %convert_element_type.120 = bf16[2048,1024]{1,0:T(8,128)(2,1)} convert(f16[2048,1024]{1,0:T(8,128)(2,1)S(1)} %all-gather.5) | non-fusion elementwise | flops 2097152 | bytes 8388608 | tf_op jit(solution)/shard_map/convert_element_type | solution.py:15
  85.6 2.0 %copy-done = bf16[2048,1024]{1,0:T(8,128)(2,1)S(1)} copy-done((bf16[2048,1024]{1,0:T(8,128)(2,1)S(1)}, bf16[2048,1024]{1,0:T(8,128)(2,1)}, u32[]{:S(2)}) %copy-start) | copy-done | bytes 4194328
  87.6 1.1 fusion.8
  89.0 0.5 fusion.4
  89.5 11.2 %collective-permute-start.1 = (bf16[136,2048]{1,0:T(8,128)(2,1)S(1)}, bf16[136,2048]{1,0:T(8,128)(2,1)S(1)}, u32[]{:S(2)}, u32[]{:S(2)}) collective-permute-start(bf16[136,2048]{1,0:T(8,128)(2,1)S(1)} %fusion.4), channel_id=1, source_target_pairs={{0,1},{1,0},{2,3},{3,2},{4,5},{5,4},{6,7},{7,6},{8,9},{9,8},{10,11... | collective-permute-start | bytes 1671176 | tf_op jit(solution)/shard_map/ppermute | solution.py:70
  100.8 1.5 collective-permute-done.1
  102.3 0.5 add_convert_fusion
  102.9 0.9 pad_maximum_fusion
  103.8 4.7 %all-to-all-start.1 = ((bf16[4,32,2176]{2,1,0:T(8,128)(2,1)}), bf16[4,32,2176]{2,1,0:T(8,128)(2,1)S(1)}, u32[]{:S(2)}, u32[]{:S(2)}) async-start(bf16[4,32,2176]{2,1,0:T(8,128)(2,1)} %pad_maximum_fusion), calls=%async_computation.1 | async-start | bytes 1114112 | tf_op jit(solution)/shard_map/all_to_all | solution.py:100
  108.6 9.2 %all-to-all-done.1 = bf16[4,32,2176]{2,1,0:T(8,128)(2,1)S(1)} async-done(((bf16[4,32,2176]{2,1,0:T(8,128)(2,1)}), bf16[4,32,2176]{2,1,0:T(8,128)(2,1)S(1)}, u32[]{:S(2)}, u32[]{:S(2)}) %all-to-all-start.1) | async-done | bytes 557088 | tf_op jit(solution)/shard_map/all_to_all | solution.py:100
  118.1 0.2 multiply_reduce_fusion
  118.5 15.2 %all-gather.6 = f16[256,2048]{1,0:T(8,128)(2,1)S(1)} all-gather(f16[32,2048]{1,0:T(8,128)(2,1)S(1)} %slice_convert_fusion), channel_id=1, replica_groups=mesh['z'=8,'y'=8,'x'=4,'core'=2] {'x','core'}, dimensions={0}, use_global_device_ids=true | all-gather | bytes 1179648 | tf_op jit(solution)/shard_map/all_gather | solution.py:111
  134.0 3.1 %fusion.11 = bf16[264,768]{1,0:T(8,128)(2,1)S(1)} fusion(bf16[2048,1024]{1,0:T(8,128)(2,1)} %all-gather.4.cloned.1.call-done, bf16[256,2048]{1,0:T(8,128)(2,1)S(1)} %convert_element_type.132, bf16[2,2048]{1,0:T(2,128)(2,1)S(1)} %slice.296, bf16[264]{0:T(512)(128)(2,1)S(1)} %pad.4.clone), kind=kOutput, calls=%fused_computation.10 | convolution fusion | flops 833918976 | bytes 4608528 | tf_op jit(solution)/shard_map/dot_general | solution.py:46
  137.5 0.5 convolution_convert_fusion
  138.0 2.1 %collective-permute-start.2 = (bf16[128,2048]{1,0:T(8,128)(2,1)S(1)}, bf16[128,2048]{1,0:T(8,128)(2,1)S(1)}, u32[]{:S(2)}, u32[]{:S(2)}) collective-permute-start(bf16[128,2048]{1,0:T(8,128)(2,1)S(1)} %convolution_convert_fusion), channel_id=1, source_target_pairs={{0,1},{1,0},{2,3},{3,2},{4,5},{5,4},{6,7},{7,6},{8,9},{9,8},{10,11... | collective-permute-start | bytes 1572872 | tf_op jit(solution)/shard_map/ppermute | solution.py:70
  140.1 1.7 %collective-permute-done.2 = bf16[128,2048]{1,0:T(8,128)(2,1)S(1)} collective-permute-done((bf16[128,2048]{1,0:T(8,128)(2,1)S(1)}, bf16[128,2048]{1,0:T(8,128)(2,1)S(1)}, u32[]{:S(2)}, u32[]{:S(2)}) %collective-permute-start.2) | collective-permute-done | bytes 524320 | tf_op jit(solution)/shard_map/ppermute | solution.py:70
  141.8 0.5 add_convert_fusion.1
  142.3 11.7 %all_to_all.20 = bf16[4,32,2048]{2,1,0:T(8,128)(2,1)S(1)} all-to-all(bf16[4,32,2048]{2,1,0:T(8,128)(2,1)S(1)} %bitcast.57), channel_id=1, replica_groups=mesh['z'=8,'y'=8,'x'=4,'core'=2] {'x'}, dimensions={0} | all-to-all | bytes 1048576 | tf_op jit(solution)/shard_map/all_to_all | solution.py:115
  154.2 0.2 multiply_reduce_fusion.1
  154.7 8.8 %all_to_all.21 = bf16[8,32,256]{2,1,0:T(8,128)(2,1)S(1)} all-to-all(bf16[8,32,256]{2,1,0:T(8,128)(2,1)S(1)} %copy.11), channel_id=1, replica_groups=mesh['z'=8,'y'=8,'x'=4,'core'=2] {'x','core'}, dimensions={0} | all-to-all | bytes 262144 | tf_op jit(solution)/shard_map/all_to_all | solution.py:119
  163.4 0.7 copy.15
  (60 shorter events, 2.3 us)
Async XLA Ops:
  6.5 127.5 %all-gather.4.cloned.1.call-start = ((), (), s32[]{:S(2)}) async-start(), calls=%async_computation.4 | async-start | bytes 4259840 | tf_op jit(solution)/shard_map/all_gather | solution.py:80
  10.1 4.9 %collective-permute-start = (bf16[16,256]{1,0:T(8,128)(2,1)S(1)}, bf16[16,256]{1,0:T(8,128)(2,1)S(1)}, u32[]{:S(2)}, u32[]{:S(2)}) collective-permute-start(bf16[16,256]{1,0:T(8,128)(2,1)S(1)} %slice.214), channel_id=1, source_target_pairs={{0,8},{8,16},{16,24},{24,32},{32,40},{40,48},{48,56},{56,64},{64,7... | collective-permute-start | bytes 24584 | tf_op jit(solution)/shard_map/ppermute | solution.py:81
  17.2 68.2 %all-to-all-start = ((bf16[8,288,256]{2,1,0:T(8,128)(2,1)}), bf16[8,288,256]{2,1,0:T(8,128)(2,1)S(1)}, u32[]{:S(2)}, u32[]{:S(2)}) async-start(bf16[8,288,256]{2,1,0:T(8,128)(2,1)} %broadcast_in_dim.41), calls=%async_computation | async-start | bytes 2359296 | tf_op jit(solution)/shard_map/all_to_all | solution.py:86
  82.1 3.2 %copy-start.2 = (f32[2,3,256]{2,0,1:T(2,128)S(1)}, f32[2,3,256]{2,0,1:T(2,128)}, u32[]{:S(2)}) copy-start(f32[2,3,256]{2,0,1:T(2,128)} %param.12) | copy-start | bytes 18436
  85.4 2.2 %copy-start = (bf16[2048,1024]{1,0:T(8,128)(2,1)S(1)}, bf16[2048,1024]{1,0:T(8,128)(2,1)}, u32[]{:S(2)}) copy-start(bf16[2048,1024]{1,0:T(8,128)(2,1)} %convert_element_type.120) | copy-start | bytes 12582916
  89.5 12.8 %collective-permute-start.1 = (bf16[136,2048]{1,0:T(8,128)(2,1)S(1)}, bf16[136,2048]{1,0:T(8,128)(2,1)S(1)}, u32[]{:S(2)}, u32[]{:S(2)}) collective-permute-start(bf16[136,2048]{1,0:T(8,128)(2,1)S(1)} %fusion.4), channel_id=1, source_target_pairs={{0,1},{1,0},{2,3},{3,2},{4,5},{5,4},{6,7},{7,6},{8,9},{9,8},{10,11... | collective-permute-start | bytes 1671176 | tf_op jit(solution)/shard_map/ppermute | solution.py:70
  103.8 14.0 %all-to-all-start.1 = ((bf16[4,32,2176]{2,1,0:T(8,128)(2,1)}), bf16[4,32,2176]{2,1,0:T(8,128)(2,1)S(1)}, u32[]{:S(2)}, u32[]{:S(2)}) async-start(bf16[4,32,2176]{2,1,0:T(8,128)(2,1)} %pad_maximum_fusion), calls=%async_computation.1 | async-start | bytes 1114112 | tf_op jit(solution)/shard_map/all_to_all | solution.py:100
  134.0 3.5 %copy-start.1 = (bf16[2048,1024]{1,0:T(8,128)(2,1)S(1)}, bf16[2048,1024]{1,0:T(8,128)(2,1)}, u32[]{:S(2)}) copy-start(bf16[2048,1024]{1,0:T(8,128)(2,1)} %all-gather.4.cloned.1.call-done) | copy-start | bytes 12582916
  138.0 3.8 %collective-permute-start.2 = (bf16[128,2048]{1,0:T(8,128)(2,1)S(1)}, bf16[128,2048]{1,0:T(8,128)(2,1)S(1)}, u32[]{:S(2)}, u32[]{:S(2)}) collective-permute-start(bf16[128,2048]{1,0:T(8,128)(2,1)S(1)} %convolution_convert_fusion), channel_id=1, source_target_pairs={{0,1},{1,0},{2,3},{3,2},{4,5},{5,4},{6,7},{7,6},{8,9},{9,8},{10,11... | collective-permute-start | bytes 1572872 | tf_op jit(solution)/shard_map/ppermute | solution.py:70
Sparse Core Ops, SparseCore 0:
  10.4 93.0 all-gather.3
where the time goes:
time: 172 us; the launch traced here: 171 us
  blocking collectives  92.5 us (54%)
  starting transfers between devices  30.1 us (18%)
  between operations  13.8 us (8%)
  waiting for transfers between devices  12.5 us (7%)
  other arithmetic  8.44 us (5%)
  local copies, waits for them, and re-layouts  7.43 us (4%)
  matrix products  6.15 us (4%)
    all_gather x1, blocking collectives, shards(): early = lax.all_gather(early, SP, axis=0, tiled=True)  56.9 us
    all_gather x1, blocking collectives, shards(): every = lax.all_gather(own.astype(jnp.float16), TP, axis=0, tiled=True)  15.2 us
    ppermute x2, starting transfers between devices, pair_sum(): got = lax.ppermute(sent, 'core', [(0, 1), (1, 0)])  13.3 us
    all_to_all x1, blocking collectives, shards(): got = lax.all_to_all(bf(branch).reshape(4, 32, D), 'x', 0, 0, tiled=True)  11.7 us
    all_to_all x1, waiting for transfers between devices, shards(): got = jnp.sum(f32(lax.all_to_all(send, 'x', 0, 0, tiled=True)), axis=0)  9.22 us
    all_to_all x1, blocking collectives, shards(): return lax.all_to_all(back, TP, 0, 0, tiled=True).reshape(256, 256)  8.78 us
    all_to_all x1, starting transfers between devices, shards(): lax.all_to_all(jnp.broadcast_to(mine[None], (8, *mine.shape)), TP, 0, 0,...  8.04 us
    all_to_all x1, starting transfers between devices, shards(): got = jnp.sum(f32(lax.all_to_all(send, 'x', 0, 0, tiled=True)), axis=0)  4.74 us
  transfers between devices with their start and end apart: 6, of which 3 were waited for; matrix products, arithmetic and copies ran while one was open for 7% of the time, Pallas kernels for 0%

commit v1 on v0

--- a/solution.py
+++ b/solution.py
@@ -86,7 +86,9 @@
     everyone = lax.all_to_all(jnp.broadcast_to(mine[None], (8, *mine.shape)), TP, 0, 0, tiled=True)
     scale = jnp.where(jnp.arange(1024) < 768, IN_UP, OUT_UP)
     early = (f32(packed(value, outer, inner, out, 0)) * scale).astype(jnp.float16)
-    early = lax.all_gather(early, SP, axis=0, tiled=True)
+    early = jnp.concatenate(
+        lax.all_to_all(jnp.stack([early] * lax.axis_size(SP)), SP, 0, 0), axis=0
+    )
     early = bf(early)
     whole = jnp.moveaxis(everyone, 0, 1).reshape(288, D)
     table = f32(whole[272:284]).reshape(3, 4, D)

time: 172 us -> 267 us (1.55)
  waiting for transfers between devices: 12.5 us -> 149 us
  blocking collectives: 92.5 us -> 37.2 us
  starting transfers between devices: 30.1 us -> 45.3 us
    all_to_all x0 -> x1, waiting for transfers between devices: none -> 101 us  [shards(): lax.all_to_all(jnp.stack([early] * lax.axis_size(SP)), SP, 0, 0)]
    all_gather x1 -> x0, blocking collectives: 56.9 us -> none  [shards(): early = lax.all_gather(early, SP, axis=0, tiled=True)]
    all_gather x1, waiting for transfers between devices: 0.02 us -> 19.4 us  [shards(): lax.all_gather(packed(value, outer, inner, out, 1), SP, axis=0, tiled=True)]
    all_to_all x1, waiting for transfers between devices: 0.01 us -> 16.3 us  [shards(): lax.all_to_all(jnp.broadcast_to(mine[None], (8, *mine.shape)), TP, 0, 0,...]
    all_to_all x0 -> x1, starting transfers between devices: none -> 16.3 us  [shards(): lax.all_to_all(jnp.stack([early] * lax.axis_size(SP)), SP, 0, 0)]
  transfers between devices with their start and end apart: 6 -> 7, of which waited for: 3 -> 6; matrix products, arithmetic and copies ran while one was open for 7% -> 4% of each run, Pallas kernels for 0% -> 0%
where the time goes in v1:
time: 267 us; the launch traced here: 266 us
  waiting for transfers between devices  149 us (56%)
  starting transfers between devices  45.3 us (17%)
  blocking collectives  37.2 us (14%)
  between operations  13.9 us (5%)
  other arithmetic  8.61 us (3%)
  matrix products  6.18 us (2%)
  local copies, waits for them, and re-layouts  5.62 us (2%)
    all_to_all x1, waiting for transfers between devices, shards(): lax.all_to_all(jnp.stack([early] * lax.axis_size(SP)), SP, 0, 0)  101 us
    all_gather x1, waiting for transfers between devices, shards(): lax.all_gather(packed(value, outer, inner, out, 1), SP, axis=0, tiled=True)  19.4 us
    all_to_all x1, waiting for transfers between devices, shards(): lax.all_to_all(jnp.broadcast_to(mine[None], (8, *mine.shape)), TP, 0, 0,...  16.3 us
    all_to_all x1, starting transfers between devices, shards(): lax.all_to_all(jnp.stack([early] * lax.axis_size(SP)), SP, 0, 0)  16.3 us
    all_gather x1, blocking collectives, shards(): every = lax.all_gather(own.astype(jnp.float16), TP, axis=0, tiled=True)  15.2 us
    all_to_all x1, blocking collectives, shards(): got = lax.all_to_all(bf(branch).reshape(4, 32, D), 'x', 0, 0, tiled=True)  12.5 us
    ppermute x2, starting transfers between devices, pair_sum(): got = lax.ppermute(sent, 'core', [(0, 1), (1, 0)])  11.1 us
    all_to_all x1, blocking collectives, shards(): return lax.all_to_all(back, TP, 0, 0, tiled=True).reshape(256, 256)  9.42 us
  transfers between devices with their start and end apart: 7, of which 6 were waited for; matrix products, arithmetic and copies ran while one was open for 4% of the time, Pallas kernels for 0%

profile of v1, /device:TPU:1, one launch (start us, length us, event | category | flops | bytes accessed | tf_op | source)
XLA Modules:
  0.0 266.0 jit_solution(17641822992023955704)
XLA Ops:
  6.5 0.7 slice.214
  7.2 4.0 %collective-permute-start = (bf16[16,256]{1,0:T(8,128)(2,1)S(1)}, bf16[16,256]{1,0:T(8,128)(2,1)S(1)}, u32[]{:S(2)}, u32[]{:S(2)}) collective-permute-start(bf16[16,256]{1,0:T(8,128)(2,1)S(1)} %slice.214), channel_id=1, source_target_pairs={{0,8},{8,16},{16,24},{24,32},{32,40},{40,48},{48,56},{56,64},{64,7... | collective-permute-start | bytes 24584 | tf_op jit(solution)/shard_map/ppermute | solution.py:81
  11.2 0.7 reduce-precision_convert_fusion.1
  12.1 1.0 maximum_maximum_fusion
  13.1 1.1 broadcast_in_dim.41
  14.2 8.2 %all-to-all-start = ((bf16[8,288,256]{2,1,0:T(8,128)(2,1)}), bf16[8,288,256]{2,1,0:T(8,128)(2,1)S(1)}, u32[]{:S(2)}, u32[]{:S(2)}) async-start(bf16[8,288,256]{2,1,0:T(8,128)(2,1)} %broadcast_in_dim.41), calls=%async_computation | async-start | bytes 2359296 | tf_op jit(solution)/shard_map/all_to_all | solution.py:86
  22.6 16.3 %all-to-all-done = bf16[8,288,256]{2,1,0:T(8,128)(2,1)S(1)} async-done(((bf16[8,288,256]{2,1,0:T(8,128)(2,1)}), bf16[8,288,256]{2,1,0:T(8,128)(2,1)S(1)}, u32[]{:S(2)}, u32[]{:S(2)}) %all-to-all-start) | async-done | bytes 1179680 | tf_op jit(solution)/shard_map/all_to_all | solution.py:86
  38.8 2.5 stack.5
  41.4 16.3 %all-to-all-start.1 = ((f16[64,32,1024]{2,1,0:T(8,128)(2,1)}), f16[64,32,1024]{2,1,0:T(8,128)(2,1)}, u32[]{:S(2)}, u32[]{:S(2)}) async-start(f16[64,32,1024]{2,1,0:T(8,128)(2,1)} %stack.5), calls=%async_computation.1 | async-start | bytes 8388608 | tf_op jit(solution)/shard_map/all_to_all | solution.py:90
  57.7 0.6 pad_maximum_fusion.6
  58.7 101.4 %all-to-all-done.1 = f16[64,32,1024]{2,1,0:T(8,128)(2,1)} async-done(((f16[64,32,1024]{2,1,0:T(8,128)(2,1)}), f16[64,32,1024]{2,1,0:T(8,128)(2,1)}, u32[]{:S(2)}, u32[]{:S(2)}) %all-to-all-start.1) | async-done | bytes 4194336 | tf_op jit(solution)/shard_map/all_to_all | solution.py:90
  160.0 3.4 %convert_element_type.127 = bf16[64,32,1024]{2,1,0:T(8,128)(2,1)S(1)} convert(f16[64,32,1024]{2,1,0:T(8,128)(2,1)} %all-to-all-done.1) | non-fusion elementwise | flops 2097152 | bytes 8388608 | tf_op jit(solution)/shard_map/convert_element_type | solution.py:15
  163.4 1.1 fusion.8
  164.8 0.5 fusion.4
  165.3 4.4 %collective-permute-start.1 = (bf16[136,2048]{1,0:T(8,128)(2,1)S(1)}, bf16[136,2048]{1,0:T(8,128)(2,1)S(1)}, u32[]{:S(2)}, u32[]{:S(2)}) collective-permute-start(bf16[136,2048]{1,0:T(8,128)(2,1)S(1)} %fusion.4), channel_id=1, source_target_pairs={{0,1},{1,0},{2,3},{3,2},{4,5},{5,4},{6,7},{7,6},{8,9},{9,8},{10,11... | collective-permute-start | bytes 1671176 | tf_op jit(solution)/shard_map/ppermute | solution.py:70
  169.8 1.5 collective-permute-done.1
  171.3 0.5 add_convert_fusion
  171.9 0.9 pad_maximum_fusion
  172.7 5.6 %all-to-all-start.2 = ((bf16[4,32,2176]{2,1,0:T(8,128)(2,1)}), bf16[4,32,2176]{2,1,0:T(8,128)(2,1)S(1)}, u32[]{:S(2)}, u32[]{:S(2)}) async-start(bf16[4,32,2176]{2,1,0:T(8,128)(2,1)} %pad_maximum_fusion), calls=%async_computation.2 | async-start | bytes 1114112 | tf_op jit(solution)/shard_map/all_to_all | solution.py:102
  178.4 9.2 %all-to-all-done.2 = bf16[4,32,2176]{2,1,0:T(8,128)(2,1)S(1)} async-done(((bf16[4,32,2176]{2,1,0:T(8,128)(2,1)}), bf16[4,32,2176]{2,1,0:T(8,128)(2,1)S(1)}, u32[]{:S(2)}, u32[]{:S(2)}) %all-to-all-start.2) | async-done | bytes 557088 | tf_op jit(solution)/shard_map/all_to_all | solution.py:102
  187.9 0.2 multiply_reduce_fusion
  188.4 15.2 %all-gather.4 = f16[256,2048]{1,0:T(8,128)(2,1)S(1)} all-gather(f16[32,2048]{1,0:T(8,128)(2,1)S(1)} %slice_convert_fusion), channel_id=1, replica_groups=mesh['z'=8,'y'=8,'x'=4,'core'=2] {'x','core'}, dimensions={0}, use_global_device_ids=true | all-gather | bytes 1179648 | tf_op jit(solution)/shard_map/all_gather | solution.py:113
  203.8 19.4 %all-gather.3.cloned.1.call-done = bf16[2048,1024]{1,0:T(8,128)(2,1)} async-done(((bf16[32,1024]{1,0:T(8,128)(2,1)}), bf16[2048,1024]{1,0:T(8,128)(2,1)}) %all-gather.3.cloned.1.call-update) | async-done | bytes 4194320 | tf_op jit(solution)/shard_map/all_gather | solution.py:80
  223.1 3.1 %fusion.11 = bf16[264,768]{1,0:T(8,128)(2,1)S(1)} fusion(bf16[2048,1024]{1,0:T(8,128)(2,1)} %all-gather.3.cloned.1.call-done, bf16[256,2048]{1,0:T(8,128)(2,1)S(1)} %convert_element_type.140, bf16[2,2048]{1,0:T(2,128)(2,1)S(1)} %slice.296, bf16[264]{0:T(512)(128)(2,1)S(1)} %pad.4.clone), kind=kOutput, calls=%fused_computation.10 | convolution fusion | flops 833918976 | bytes 4608528 | tf_op jit(solution)/shard_map/dot_general | solution.py:46
  226.7 0.5 convolution_convert_fusion
  227.2 6.7 %collective-permute-start.2 = (bf16[128,2048]{1,0:T(8,128)(2,1)S(1)}, bf16[128,2048]{1,0:T(8,128)(2,1)S(1)}, u32[]{:S(2)}, u32[]{:S(2)}) collective-permute-start(bf16[128,2048]{1,0:T(8,128)(2,1)S(1)} %convolution_convert_fusion), channel_id=1, source_target_pairs={{0,1},{1,0},{2,3},{3,2},{4,5},{5,4},{6,7},{7,6},{8,9},{9,8},{10,11... | collective-permute-start | bytes 1572872 | tf_op jit(solution)/shard_map/ppermute | solution.py:70
  233.9 1.5 collective-permute-done.2
  235.4 0.5 add_convert_fusion.1
  235.9 12.5 %all_to_all.25 = bf16[4,32,2048]{2,1,0:T(8,128)(2,1)S(1)} all-to-all(bf16[4,32,2048]{2,1,0:T(8,128)(2,1)S(1)} %bitcast.61), channel_id=1, replica_groups=mesh['z'=8,'y'=8,'x'=4,'core'=2] {'x'}, dimensions={0} | all-to-all | bytes 1048576 | tf_op jit(solution)/shard_map/all_to_all | solution.py:117
  248.7 0.2 multiply_reduce_fusion.1
  249.1 9.4 %all_to_all.26 = bf16[8,32,256]{2,1,0:T(8,128)(2,1)S(1)} all-to-all(bf16[8,32,256]{2,1,0:T(8,128)(2,1)S(1)} %copy.11), channel_id=1, replica_groups=mesh['z'=8,'y'=8,'x'=4,'core'=2] {'x','core'}, dimensions={0} | all-to-all | bytes 262144 | tf_op jit(solution)/shard_map/all_to_all | solution.py:121
  258.5 0.7 copy.15
  (68 shorter events, 2.4 us)
Async XLA Ops:
  7.2 4.9 %collective-permute-start = (bf16[16,256]{1,0:T(8,128)(2,1)S(1)}, bf16[16,256]{1,0:T(8,128)(2,1)S(1)}, u32[]{:S(2)}, u32[]{:S(2)}) collective-permute-start(bf16[16,256]{1,0:T(8,128)(2,1)S(1)} %slice.214), channel_id=1, source_target_pairs={{0,8},{8,16},{16,24},{24,32},{32,40},{40,48},{48,56},{56,64},{64,7... | collective-permute-start | bytes 24584 | tf_op jit(solution)/shard_map/ppermute | solution.py:81
  14.2 8.2 %copy-start.1 = (bf16[2,32,256]{2,1,0:T(8,128)(2,1)S(1)}, bf16[2,32,256]{2,1,0:T(8,128)(2,1)}, u32[]{:S(2)}) copy-start(bf16[2,32,256]{2,1,0:T(8,128)(2,1)} %param.9) | copy-start | bytes 98308
  14.2 8.3 %copy-start.2 = (bf16[2,256,32]{1,2,0:T(8,128)(2,1)S(1)}, bf16[2,256,32]{1,2,0:T(8,128)(2,1)}, u32[]{:S(2)}) copy-start(bf16[2,256,32]{1,2,0:T(8,128)(2,1)} %param.13) | copy-start | bytes 98308
  14.2 8.3 %copy-start.3 = (bf16[2,32,256]{2,1,0:T(8,128)(2,1)S(1)}, bf16[2,32,256]{2,1,0:T(8,128)(2,1)}, u32[]{:S(2)}) copy-start(bf16[2,32,256]{2,1,0:T(8,128)(2,1)} %param.11) | copy-start | bytes 98308
  14.2 8.3 %copy-start.4 = (bf16[2,32,256]{2,1,0:T(8,128)(2,1)S(1)}, bf16[2,32,256]{2,1,0:T(8,128)(2,1)}, u32[]{:S(2)}) copy-start(bf16[2,32,256]{2,1,0:T(8,128)(2,1)} %param.10) | copy-start | bytes 98308
  14.2 24.6 %all-to-all-start = ((bf16[8,288,256]{2,1,0:T(8,128)(2,1)}), bf16[8,288,256]{2,1,0:T(8,128)(2,1)S(1)}, u32[]{:S(2)}, u32[]{:S(2)}) async-start(bf16[8,288,256]{2,1,0:T(8,128)(2,1)} %broadcast_in_dim.41), calls=%async_computation | async-start | bytes 2359296 | tf_op jit(solution)/shard_map/all_to_all | solution.py:86
  41.4 17.1 %copy-start.5 = (f32[2,3,256]{2,0,1:T(2,128)S(1)}, f32[2,3,256]{2,0,1:T(2,128)}, u32[]{:S(2)}) copy-start(f32[2,3,256]{2,0,1:T(2,128)} %param.12) | copy-start | bytes 18436
  41.4 118.7 %all-to-all-start.1 = ((f16[64,32,1024]{2,1,0:T(8,128)(2,1)}), f16[64,32,1024]{2,1,0:T(8,128)(2,1)}, u32[]{:S(2)}, u32[]{:S(2)}) async-start(f16[64,32,1024]{2,1,0:T(8,128)(2,1)} %stack.5), calls=%async_computation.1 | async-start | bytes 8388608 | tf_op jit(solution)/shard_map/all_to_all | solution.py:90
  57.6 165.5 %all-gather.3.cloned.1.call-start = ((), (), s32[]{:S(2)}) async-start(), calls=%async_computation.5 | async-start | bytes 4259840 | tf_op jit(solution)/shard_map/all_gather | solution.py:80
  165.3 6.0 %collective-permute-start.1 = (bf16[136,2048]{1,0:T(8,128)(2,1)S(1)}, bf16[136,2048]{1,0:T(8,128)(2,1)S(1)}, u32[]{:S(2)}, u32[]{:S(2)}) collective-permute-start(bf16[136,2048]{1,0:T(8,128)(2,1)S(1)} %fusion.4), channel_id=1, source_target_pairs={{0,1},{1,0},{2,3},{3,2},{4,5},{5,4},{6,7},{7,6},{8,9},{9,8},{10,11... | collective-permute-start | bytes 1671176 | tf_op jit(solution)/shard_map/ppermute | solution.py:70
  172.7 14.9 %all-to-all-start.2 = ((bf16[4,32,2176]{2,1,0:T(8,128)(2,1)}), bf16[4,32,2176]{2,1,0:T(8,128)(2,1)S(1)}, u32[]{:S(2)}, u32[]{:S(2)}) async-start(bf16[4,32,2176]{2,1,0:T(8,128)(2,1)} %pad_maximum_fusion), calls=%async_computation.2 | async-start | bytes 1114112 | tf_op jit(solution)/shard_map/all_to_all | solution.py:102
  223.1 3.5 %copy-start = (bf16[2048,1024]{1,0:T(8,128)(2,1)S(1)}, bf16[2048,1024]{1,0:T(8,128)(2,1)}, u32[]{:S(2)}) copy-start(bf16[2048,1024]{1,0:T(8,128)(2,1)} %all-gather.3.cloned.1.call-done) | copy-start | bytes 12582916
  227.2 8.2 %collective-permute-start.2 = (bf16[128,2048]{1,0:T(8,128)(2,1)S(1)}, bf16[128,2048]{1,0:T(8,128)(2,1)S(1)}, u32[]{:S(2)}, u32[]{:S(2)}) collective-permute-start(bf16[128,2048]{1,0:T(8,128)(2,1)S(1)} %convolution_convert_fusion), channel_id=1, source_target_pairs={{0,1},{1,0},{2,3},{3,2},{4,5},{5,4},{6,7},{7,6},{8,9},{9,8},{10,11... | collective-permute-start | bytes 1572872 | tf_op jit(solution)/shard_map/ppermute | solution.py:70
Sparse Core Ops, SparseCore 0:
  61.5 161.5 all-gather.2
